TPU v7x, 32 devices: a whole 2x2x4 slice. The times are simulated.
32 devices in a mesh: sp: 8 (over z, y), tp: 4 (over x, core).
Axes of the slice: x: 2, y: 2, z: 4, core: 2. Of those that a mesh axis runs over, the one named last changes fastest.
Arguments:
- stream: bfloat16 [2048, 2048], P('sp', 'tp'), may hold values from -8 to 8
- norm_gain: float32 [2, 2048], P(None, 'tp'), may hold values from 0.1 to 1.9
- query_weight: bfloat16 [2, 2048, 1024], P(None, None, 'tp'), may hold values from -4 to 4
- key_weight: bfloat16 [2, 2048, 1024], P(None, None, 'tp'), may hold values from -4 to 4
- value_weight: bfloat16 [2, 2048, 1024], P(None, None, 'tp'), may hold values from -0.125 to 0.125
- out_weight: bfloat16 [2, 1024, 2048], P(None, None, 'tp'), may hold values from -1.5 to 1.5
- rel_bias: float32 [2, 16, 257], P(None, 'tp'), may hold values from -4 to 4
Outputs:
- mixed: bfloat16 [2048, 2048], P('sp', 'tp')
All inputs are finite; a program needn't handle non-finite values.
Results may differ from a plain program's by a relative error of at most 0.013.
Values may be sent and summed in bfloat16 or wider, within the bound.
A program may use at most 64 MiB of HBM per device.

v0:
```python
import jax
import jax.numpy as jnp
from jax import lax
from jax.sharding import PartitionSpec as P

D = 2048
SEG = 64
PREV = 8
CLIP = 128
LAYERS = 2


epsilon = 1e-06
masked_score = -1e30


def from_behind(shard, axis, by):
    count = lax.axis_size(axis)
    pairs = [(i, i + by) for i in range(count) if 0 <= i + by < count]
    return lax.ppermute(shard, axis, pairs)


def normalize(residual, gain):
    values_f = residual.astype(jnp.float32)
    squares = lax.psum(jnp.sum(values_f * values_f, axis=-1, keepdims=True), "tp")
    scaled = values_f * lax.rsqrt(squares / D + epsilon)
    return (scaled * gain).astype(jnp.bfloat16)


def bias_table(table, band_len):
    heads_here = table.shape[0]
    near_part = table[:, CLIP - (SEG - 1) :]
    far_count = band_len - 1 - CLIP
    far_part = jnp.broadcast_to(table[:, 2 * CLIP : 2 * CLIP + 1], (heads_here, far_count))
    reversed_row = jnp.concatenate([near_part, far_part], axis=1)[:, ::-1]
    slices = [
        reversed_row[:, SEG - 1 - within : SEG - 1 - within + band_len] for within in range(SEG)
    ]
    return jnp.stack(slices, axis=1)


def project_rows(rows_local, query_count, query_mat, key_mat, value_mat):
    row_count = rows_local.shape[0]
    first_query = row_count - query_count
    piece = lax.all_gather(rows_local, "tp", axis=1, tiled=True)
    query_sum = jnp.dot(piece[first_query:], query_mat, preferred_element_type=jnp.float32)
    key_sum = jnp.dot(piece, key_mat, preferred_element_type=jnp.float32)
    value_sum = jnp.dot(piece, value_mat, preferred_element_type=jnp.float32)
    return (
        query_sum.astype(jnp.bfloat16),
        key_sum.astype(jnp.bfloat16),
        value_sum.astype(jnp.bfloat16),
    )


def earlier_inputs(normed, shift_count):
    pieces = [from_behind(normed, "sp", step_back) for step_back in range(shift_count, 0, -1)]
    return jnp.concatenate(pieces, axis=0)


def band_blocks(extended, segments):
    blocked = extended.reshape((segments + PREV, SEG) + extended.shape[1:])
    return jnp.concatenate(
        [blocked[offset_seg : offset_seg + segments] for offset_seg in range(PREV + 1)], axis=1
    )


def attend(query_rows, key_ext, value_ext, position_bias, visible):
    tok_rows, head_cols = query_rows.shape
    heads_here = position_bias.shape[0]
    head_dim = head_cols // heads_here
    segments = tok_rows // SEG
    band_len = (PREV + 1) * SEG
    query_blocks = query_rows.reshape(segments, SEG, heads_here, head_dim)
    key_blocks = band_blocks(key_ext, segments).reshape(segments, band_len, heads_here, head_dim)
    value_blocks = band_blocks(value_ext, segments).reshape(
        segments, band_len, heads_here, head_dim
    )
    visible_blocks = band_blocks(visible, segments)
    scores = jnp.einsum(
        "sqhd,skhd->hsqk", query_blocks, key_blocks, preferred_element_type=jnp.float32
    )
    scores = scores * head_dim ** (-0.5) + position_bias[:, None]
    scores = jnp.where(visible_blocks[None, :, None, :], scores, masked_score)
    maximum = jnp.max(scores, axis=-1, keepdims=True)
    exponent = jnp.exp(scores - maximum)
    weights = (exponent / jnp.sum(exponent, axis=-1, keepdims=True)).astype(jnp.bfloat16)
    attended = jnp.einsum(
        "hsqk,skhd->sqhd", weights, value_blocks, preferred_element_type=jnp.float32
    )
    return attended.astype(jnp.bfloat16).reshape(tok_rows, head_cols)


def per_device(stream, norm_gain, query_weight, key_weight, value_weight, out_weight, rel_bias):
    tok_rows = stream.shape[0]
    reach_rows = PREV * SEG
    shift_count = max(1, reach_rows // tok_rows)
    band_len = reach_rows + SEG
    positions = (
        lax.axis_index("sp") * tok_rows
        - reach_rows
        + jnp.arange(reach_rows + tok_rows, dtype=jnp.int32)
    )
    visible = positions >= 0
    residual = stream
    for layer_index in range(LAYERS):
        normed = normalize(residual, norm_gain[layer_index])
        normed_ext = jnp.concatenate([earlier_inputs(normed, shift_count), normed], axis=0)
        query_rows, key_ext, value_ext = project_rows(
            normed_ext,
            tok_rows,
            query_weight[layer_index],
            key_weight[layer_index],
            value_weight[layer_index],
        )
        position_bias = bias_table(rel_bias[layer_index], band_len)
        attended = attend(query_rows, key_ext, value_ext, position_bias, visible)
        out_mat = out_weight[layer_index]
        summed = residual.astype(jnp.float32) + jnp.dot(
            lax.all_gather(attended, "tp", axis=1, tiled=True),
            out_mat,
            preferred_element_type=jnp.float32,
        )
        residual = summed.astype(jnp.bfloat16)
    return residual


def solution(mesh):
    placed = (
        P("sp", "tp"),
        P(None, "tp"),
        P(None, None, "tp"),
        P(None, None, "tp"),
        P(None, None, "tp"),
        P(None, None, "tp"),
        P(None, "tp", None),
    )
    return jax.shard_map(
        per_device, mesh=mesh, in_specs=placed, out_specs=P("sp", "tp"), check_vma=False
    )
```

profile of v0, /device:TPU:9, one launch (start us, length us, event | category | flops | bytes accessed | tf_op | source)
XLA Modules:
  0.0 261.5 jit_solution(17611809908315193769)
XLA Ops:
  7.6 5.7 %psum.14 = f32[256,1]{0,1:T(1,128)S(1)} all-reduce(f32[256,1]{0,1:T(1,128)S(1)} %bitcast.562), channel_id=1, replica_groups=mesh['sp'=8,'tp'=4] {'tp'}, use_global_device_ids=true, to_apply=%region_1.0 | all-reduce | flops 256 | bytes 2048 | tf_op jit(solution)/shard_map/psum | solution.py:25
  15.2 3.1 %collective-permute-start.1 = (bf16[256,512]{1,0:T(8,128)(2,1)S(1)}, bf16[256,512]{1,0:T(8,128)(2,1)S(1)}, u32[]{:S(2)}, u32[]{:S(2)}) collective-permute-start(bf16[256,512]{1,0:T(8,128)(2,1)S(1)} %fusion.51), channel_id=1, source_target_pairs={{0,4},{4,8},{8,12},{12,16},{16,20},{20,24},{24,28},{1,5},{5,9},{9,... | collective-permute-start | bytes 786440 | tf_op jit(solution)/shard_map/ppermute | solution.py:20
  18.3 3.2 %collective-permute-start = (bf16[256,512]{1,0:T(8,128)(2,1)S(1)}, bf16[256,512]{1,0:T(8,128)(2,1)S(1)}, u32[]{:S(2)}, u32[]{:S(2)}) collective-permute-start(bf16[256,512]{1,0:T(8,128)(2,1)S(1)} %fusion.51), channel_id=1, source_target_pairs={{0,8},{4,12},{8,16},{12,20},{16,24},{20,28},{1,9},{5,13},{9,17},{1... | collective-permute-start | bytes 786440 | tf_op jit(solution)/shard_map/ppermute | solution.py:20
  95.1 6.1 %stack.454 = f32[4,64,576]{2,1,0:T(8,128)} concatenate(f32[4,1,576]{2,1,0:T(1,128)S(1)} %copy.193, f32[4,1,576]{2,1,0:T(1,128)S(1)} %copy.194, f32[4,1,576]{2,1,0:T(1,128)S(1)} %copy.195, f32[4,1,576]{2,1,0:T(1,128)S(1)} %copy.196, f32[4,1,576]{2,1,0:T(1,128)S(1)} %copy.197, f32[4,1,576]{2,1,0:T(1,128)S(1)} %copy.198, f32[4,1,576]{2,1,0:T(1,128)S(1)} %copy.199, ...), dimensions={1} | concatenate | bytes 1179648 | tf_op jit(solution)/shard_map/stack | solution.py:39
  115.2 2.1 convolution_convert_fusion.5
  118.3 2.2 convolution_convert_fusion.3
  124.6 3.2 %convolution_convert_fusion.2 = bf16[768,256]{1,0:T(8,128)(2,1)S(1)} fusion(bf16[768,2048]{1,0:T(8,128)(2,1)} %all-gather.3.cloned.1.call-done, bf16[2,2048,256]{2,1,0:T(8,128)(2,1)} %param.10), kind=kOutput, calls=%fused_computation.24 | convolution fusion | flops 805502976 | bytes 4587520 | tf_op jit(solution)/shard_map/dot_general | solution.py:47
  137.5 2.8 %concatenate.125 = bf16[4,576,4,64]{1,3,0,2:T(8,128)(2,1)S(1)} concatenate(bf16[4,64,4,64]{1,3,0,2:T(8,128)(2,1)} %copy.183, bf16[4,64,4,64]{1,3,0,2:T(8,128)(2,1)} %copy.184, bf16[4,64,4,64]{1,3,0,2:T(8,128)(2,1)} %copy.185, bf16[4,64,4,64]{1,3,0,2:T(8,128)(2,1)} %copy.186, bf16[4,64,4,64]{1,3,0,2:T(8,128)(2,1)} %copy.187, bf16[4,64,4,64]{1,3,0,2:T(8,128)(2,1)} %copy.188, ...), dimensions={1} | concatenate | bytes 2359296 | tf_op jit(solution)/shard_map/concatenate | solution.py:63
  140.4 3.7 %fusion.204 = (f32[4,4,64]{2,1,0:T(4,128)S(1)}, f32[4,4,64,576]{3,2,1,0:T(8,128)}) fusion(f32[4,64,576]{2,1,0:T(8,128)} %stack.454, pred[4,576]{1,0:T(4,128)(4,1)S(1)} %copy-done.42, bf16[4,576,4,64]{1,3,0,2:T(8,128)(2,1)S(1)} %concatenate.125, bf16[4,64,4,64]{3,2,1,0:T(4,128)(2,1)} %reshape.164), kind=kOutput, calls=%fused_computation.465 | convolution fusion | flops 78447168 | bytes 4266240 | tf_op jit(solution)/shard_map/sub | solution.py:86
  144.0 2.3 concatenate.114
  146.4 2.4 fusion.28
  149.4 8.9 %all_gather.13 = bf16[256,1024]{1,0:T(8,128)(2,1)S(1)} all-gather(bf16[256,256]{1,0:T(8,128)(2,1)S(1)} %reshape.165), channel_id=1, replica_groups=mesh['sp'=8,'tp'=4] {'tp'}, dimensions={1}, use_global_device_ids=true | all-gather | bytes 655360 | tf_op jit(solution)/shard_map/all_gather | solution.py:120
  160.3 5.2 %psum.15 = f32[256,1]{0,1:T(1,128)S(1)} all-reduce(f32[256,1]{0,1:T(1,128)S(1)} %bitcast.563), channel_id=1, replica_groups=mesh['sp'=8,'tp'=4] {'tp'}, use_global_device_ids=true, to_apply=%region_5.6 | all-reduce | flops 256 | bytes 2048 | tf_op jit(solution)/shard_map/psum | solution.py:25
  165.6 3.1 %collective-permute-start.3 = (bf16[256,512]{1,0:T(8,128)(2,1)S(1)}, bf16[256,512]{1,0:T(8,128)(2,1)S(1)}, u32[]{:S(2)}, u32[]{:S(2)}) collective-permute-start(bf16[256,512]{1,0:T(8,128)(2,1)S(1)} %multiply_convert_fusion), channel_id=1, source_target_pairs={{0,4},{4,8},{8,12},{12,16},{16,20},{20,24},{24,28},{1,5},{5,9},{9,... | collective-permute-start | bytes 786440 | tf_op jit(solution)/shard_map/ppermute | solution.py:20
  190.6 6.1 %stack.519 = f32[4,64,576]{2,1,0:T(8,128)} concatenate(f32[4,1,576]{2,1,0:T(1,128)S(1)} %copy.277, f32[4,1,576]{2,1,0:T(1,128)S(1)} %copy.278, f32[4,1,576]{2,1,0:T(1,128)S(1)} %copy.279, f32[4,1,576]{2,1,0:T(1,128)S(1)} %copy.280, f32[4,1,576]{2,1,0:T(1,128)S(1)} %copy.281, f32[4,1,576]{2,1,0:T(1,128)S(1)} %copy.282, f32[4,1,576]{2,1,0:T(1,128)S(1)} %copy.283, ...), dimensions={1} | concatenate | bytes 1179648 | tf_op jit(solution)/shard_map/stack | solution.py:39
  196.7 14.4 %all-gather.5.cloned.1.call-done = bf16[768,2048]{1,0:T(8,128)(2,1)} async-done(((bf16[768,512]{1,0:T(8,128)(2,1)}), bf16[768,2048]{1,0:T(8,128)(2,1)}) %all-gather.5.cloned.1.call-update) | async-done | bytes 3145744 | tf_op jit(solution)/shard_map/all_gather | solution.py:45
  214.1 2.2 convolution_convert_fusion.1
  220.4 3.2 %convolution_convert_fusion = bf16[768,256]{1,0:T(8,128)(2,1)S(1)} fusion(bf16[768,2048]{1,0:T(8,128)(2,1)} %all-gather.5.cloned.1.call-done, bf16[2,2048,256]{2,1,0:T(8,128)(2,1)} %param.10), kind=kOutput, calls=%fused_computation.22 | convolution fusion | flops 805502976 | bytes 4587520 | tf_op jit(solution)/shard_map/dot_general | solution.py:47
  233.4 2.8 %concatenate.147 = bf16[4,576,4,64]{1,3,0,2:T(8,128)(2,1)S(1)} concatenate(bf16[4,64,4,64]{1,3,0,2:T(8,128)(2,1)} %copy.267, bf16[4,64,4,64]{1,3,0,2:T(8,128)(2,1)} %copy.268, bf16[4,64,4,64]{1,3,0,2:T(8,128)(2,1)} %copy.269, bf16[4,64,4,64]{1,3,0,2:T(8,128)(2,1)} %copy.270, bf16[4,64,4,64]{1,3,0,2:T(8,128)(2,1)} %copy.271, bf16[4,64,4,64]{1,3,0,2:T(8,128)(2,1)} %copy.272, ...), dimensions={1} | concatenate | bytes 2359296 | tf_op jit(solution)/shard_map/concatenate | solution.py:63
  236.2 3.7 %fusion.207 = (f32[4,4,64]{2,1,0:T(4,128)S(1)}, f32[4,4,64,576]{3,2,1,0:T(8,128)}) fusion(f32[4,64,576]{2,1,0:T(8,128)} %stack.519, pred[4,576]{1,0:T(4,128)(4,1)S(1)} %copy-done.43, bf16[4,576,4,64]{1,3,0,2:T(8,128)(2,1)S(1)} %concatenate.147, bf16[4,64,4,64]{3,2,1,0:T(4,128)(2,1)} %reshape.166), kind=kOutput, calls=%fused_computation.466 | convolution fusion | flops 78447168 | bytes 4266240 | tf_op jit(solution)/shard_map/sub | solution.py:86
  239.9 2.3 concatenate.137
  242.2 2.4 fusion.25
  245.1 7.3 %all_gather.15 = bf16[256,1024]{1,0:T(8,128)(2,1)S(1)} all-gather(bf16[256,256]{1,0:T(8,128)(2,1)S(1)} %reshape.167), channel_id=1, replica_groups=mesh['sp'=8,'tp'=4] {'tp'}, dimensions={1}, use_global_device_ids=true | all-gather | bytes 655360 | tf_op jit(solution)/shard_map/all_gather | solution.py:120
  252.3 2.4 fusion.17
  (603 shorter events, 145.1 us)
Async XLA Ops:
  6.5 108.7 %all-gather.3.cloned.1.call-start = ((), (), s32[]{:S(2)}) async-start(), calls=%async_computation | async-start | bytes 3932160 | tf_op jit(solution)/shard_map/all_gather | solution.py:45
  15.2 69.4 %collective-permute-start.1 = (bf16[256,512]{1,0:T(8,128)(2,1)S(1)}, bf16[256,512]{1,0:T(8,128)(2,1)S(1)}, u32[]{:S(2)}, u32[]{:S(2)}) collective-permute-start(bf16[256,512]{1,0:T(8,128)(2,1)S(1)} %fusion.51), channel_id=1, source_target_pairs={{0,4},{4,8},{8,12},{12,16},{16,20},{20,24},{24,28},{1,5},{5,9},{9,... | collective-permute-start | bytes 786440 | tf_op jit(solution)/shard_map/ppermute | solution.py:20
  18.3 66.3 %collective-permute-start = (bf16[256,512]{1,0:T(8,128)(2,1)S(1)}, bf16[256,512]{1,0:T(8,128)(2,1)S(1)}, u32[]{:S(2)}, u32[]{:S(2)}) collective-permute-start(bf16[256,512]{1,0:T(8,128)(2,1)S(1)} %fusion.51), channel_id=1, source_target_pairs={{0,8},{4,12},{8,16},{12,20},{16,24},{20,28},{1,9},{5,13},{9,17},{1... | collective-permute-start | bytes 786440 | tf_op jit(solution)/shard_map/ppermute | solution.py:20
  85.6 125.5 %all-gather.5.cloned.1.call-start = ((), (), s32[]{:S(2)}) async-start(), calls=%async_computation.1 | async-start | bytes 3932160 | tf_op jit(solution)/shard_map/all_gather | solution.py:45
  149.2 21.6 %copy-start.27 = (f32[4,640]{1,0:T(4,128)S(1)}, f32[4,640]{1,0:T(4,128)}, u32[]{:S(2)}) copy-start(f32[4,640]{1,0:T(4,128)} %reverse.211) | copy-start | bytes 30724
  149.2 21.7 %copy-start.7 = (f32[4,1,576]{2,0,1:T(4,128)S(1)}, f32[4,1,576]{2,0,1:T(4,128)}, u32[]{:S(2)}) copy-start(f32[4,1,576]{2,0,1:T(4,128)} %slice_bitcast_fusion.8) | copy-start | bytes 27652
  149.2 21.7 %copy-start.8 = (f32[4,1,576]{2,0,1:T(4,128)S(1)}, f32[4,1,576]{2,0,1:T(4,128)}, u32[]{:S(2)}) copy-start(f32[4,1,576]{2,0,1:T(4,128)} %slice_bitcast_fusion.7) | copy-start | bytes 27652
  149.2 21.7 %copy-start.9 = (f32[4,1,576]{2,0,1:T(4,128)S(1)}, f32[4,1,576]{2,0,1:T(4,128)}, u32[]{:S(2)}) copy-start(f32[4,1,576]{2,0,1:T(4,128)} %slice_bitcast_fusion.16) | copy-start | bytes 27652
  149.2 21.7 %copy-start.10 = (f32[4,1,576]{2,0,1:T(4,128)S(1)}, f32[4,1,576]{2,0,1:T(4,128)}, u32[]{:S(2)}) copy-start(f32[4,1,576]{2,0,1:T(4,128)} %slice_bitcast_fusion.15) | copy-start | bytes 27652
  149.3 21.7 %copy-start.11 = (f32[4,1,576]{2,0,1:T(4,128)S(1)}, f32[4,1,576]{2,0,1:T(4,128)}, u32[]{:S(2)}) copy-start(f32[4,1,576]{2,0,1:T(4,128)} %slice_bitcast_fusion.14) | copy-start | bytes 27652
  149.3 21.8 %copy-start.12 = (f32[4,1,576]{2,0,1:T(4,128)S(1)}, f32[4,1,576]{2,0,1:T(4,128)}, u32[]{:S(2)}) copy-start(f32[4,1,576]{2,0,1:T(4,128)} %slice_bitcast_fusion.13) | copy-start | bytes 27652
  149.3 21.8 %copy-start.13 = (f32[4,1,576]{2,0,1:T(4,128)S(1)}, f32[4,1,576]{2,0,1:T(4,128)}, u32[]{:S(2)}) copy-start(f32[4,1,576]{2,0,1:T(4,128)} %slice_bitcast_fusion.12) | copy-start | bytes 27652
  149.3 21.8 %copy-start.14 = (f32[4,1,576]{2,0,1:T(4,128)S(1)}, f32[4,1,576]{2,0,1:T(4,128)}, u32[]{:S(2)}) copy-start(f32[4,1,576]{2,0,1:T(4,128)} %slice_bitcast_fusion.11) | copy-start | bytes 27652
  149.3 21.8 %copy-start.15 = (f32[4,1,576]{2,0,1:T(4,128)S(1)}, f32[4,1,576]{2,0,1:T(4,128)}, u32[]{:S(2)}) copy-start(f32[4,1,576]{2,0,1:T(4,128)} %slice_bitcast_fusion.10) | copy-start | bytes 27652
  149.3 21.8 %copy-start.16 = (f32[4,1,576]{2,0,1:T(4,128)S(1)}, f32[4,1,576]{2,0,1:T(4,128)}, u32[]{:S(2)}) copy-start(f32[4,1,576]{2,0,1:T(4,128)} %slice_bitcast_fusion.9) | copy-start | bytes 27652
  149.3 21.9 %copy-start.17 = (f32[4,1,576]{2,0,1:T(4,128)S(1)}, f32[4,1,576]{2,0,1:T(4,128)}, u32[]{:S(2)}) copy-start(f32[4,1,576]{2,0,1:T(4,128)} %slice_bitcast_fusion.6) | copy-start | bytes 27652
  149.3 21.9 %copy-start.18 = (f32[4,1,576]{2,0,1:T(4,128)S(1)}, f32[4,1,576]{2,0,1:T(4,128)}, u32[]{:S(2)}) copy-start(f32[4,1,576]{2,0,1:T(4,128)} %slice_bitcast_fusion.24) | copy-start | bytes 27652
  149.3 21.9 %copy-start.19 = (f32[4,1,576]{2,0,1:T(4,128)S(1)}, f32[4,1,576]{2,0,1:T(4,128)}, u32[]{:S(2)}) copy-start(f32[4,1,576]{2,0,1:T(4,128)} %slice_bitcast_fusion.23) | copy-start | bytes 27652
  149.3 21.9 %copy-start.20 = (f32[4,1,576]{2,0,1:T(4,128)S(1)}, f32[4,1,576]{2,0,1:T(4,128)}, u32[]{:S(2)}) copy-start(f32[4,1,576]{2,0,1:T(4,128)} %slice_bitcast_fusion.22) | copy-start | bytes 27652
  149.4 21.9 %copy-start.21 = (f32[4,1,576]{2,0,1:T(4,128)S(1)}, f32[4,1,576]{2,0,1:T(4,128)}, u32[]{:S(2)}) copy-start(f32[4,1,576]{2,0,1:T(4,128)} %slice_bitcast_fusion.21) | copy-start | bytes 27652
  149.4 22.0 %copy-start.22 = (f32[4,1,576]{2,0,1:T(4,128)S(1)}, f32[4,1,576]{2,0,1:T(4,128)}, u32[]{:S(2)}) copy-start(f32[4,1,576]{2,0,1:T(4,128)} %slice_bitcast_fusion.20) | copy-start | bytes 27652
  160.3 19.4 %copy-start.1 = (f32[256,512]{1,0:T(8,128)}, f32[256,512]{1,0:T(8,128)S(1)}, u32[]{:S(2)}) copy-start(f32[256,512]{1,0:T(8,128)S(1)} %get-tuple-element.183) | copy-start | bytes 1572868
  165.6 12.5 %collective-permute-start.3 = (bf16[256,512]{1,0:T(8,128)(2,1)S(1)}, bf16[256,512]{1,0:T(8,128)(2,1)S(1)}, u32[]{:S(2)}, u32[]{:S(2)}) collective-permute-start(bf16[256,512]{1,0:T(8,128)(2,1)S(1)} %multiply_convert_fusion), channel_id=1, source_target_pairs={{0,4},{4,8},{8,12},{12,16},{16,20},{20,24},{24,28},{1,5},{5,9},{9,... | collective-permute-start | bytes 786440 | tf_op jit(solution)/shard_map/ppermute | solution.py:20
  168.8 9.4 %collective-permute-start.2 = (bf16[256,512]{1,0:T(8,128)(2,1)S(1)}, bf16[256,512]{1,0:T(8,128)(2,1)S(1)}, u32[]{:S(2)}, u32[]{:S(2)}) collective-permute-start(bf16[256,512]{1,0:T(8,128)(2,1)S(1)} %multiply_convert_fusion), channel_id=1, source_target_pairs={{0,8},{4,12},{8,16},{12,20},{16,24},{20,28},{1,9},{5,13},{9,17},{1... | collective-permute-start | bytes 786440 | tf_op jit(solution)/shard_map/ppermute | solution.py:20
  (28 other events, 344.8 us)
Sparse Core Ops, SparseCore 0:
  85.7 28.9 all-gather.2
  179.3 31.7 all-gather.4
where the time goes:
time: 264 us; the launch traced here: 262 us
  local copies, waits for them, and re-layouts  155 us (59%)
  matrix products  31.3 us (12%)
  blocking collectives  27.1 us (10%)
  between operations  15.7 us (6%)
  waiting for transfers between devices  14.4 us (5%)
  starting transfers between devices  11.7 us (4%)
  other arithmetic  6.69 us (3%)
    unnamed x222, local copies, waits for them, and re-layouts  59.2 us
    another operation x256, local copies, waits for them, and re-layouts, bias_table(): return jnp.stack(slices, axis=1)  52.5 us
    concatenate x77, local copies, waits for them, and re-layouts, band_blocks(): jnp.concatenate([blocked[offset_seg:offset_seg + segments] for offset_seg...  37.9 us
    all_gather x2, blocking collectives, per_device(): lax.all_gather(attended, 'tp', axis=1, tiled=True)  16.2 us
    all_gather x2, waiting for transfers between devices, project_rows(): piece = lax.all_gather(rows_local, 'tp', axis=1, tiled=True)  14.4 us
    ppermute x4, starting transfers between devices, from_behind(): return lax.ppermute(shard, axis, pairs)  11.5 us
    psum x2, blocking collectives, normalize(): lax.psum(jnp.sum(values_f * values_f, axis=-1, keepdims=True), 'tp')  10.9 us
    sub x2, matrix products, attend(): exponent = jnp.exp(scores - maximum)  7.34 us
  transfers between devices with their start and end apart: 6, of which 1 were waited for; matrix products, arithmetic and copies ran while one was open for 44% of the time, Pallas kernels for 0%

commit v1 on v0

v1 whole, which is shorter than its diff:
```python
import functools

import jax
import jax.numpy as jnp
from jax import lax
from jax.experimental import pallas as pl
from jax.experimental.pallas import tpu as pltpu
from jax.sharding import PartitionSpec as P

SEG = 64
PREV = 8
CLIP = 128
LANES = 128
CHUNKS = 4
PAIR = 2 * SEG
REACH = PREV * SEG
BAND = REACH + PAIR

epsilon = 1e-06
masked_score = -1e30
MESH = pl.DeviceIdType.MESH


class Gather:
    def __init__(self, n_tp, slot, send_sems, recv_sems):
        self.n_x = n_tp // 2
        self.me = lax.axis_index("tp")
        self.core = lax.rem(self.me, 2)
        self.x = self.me // 2
        self.sibling = self.me + 1 - 2 * self.core
        self.slot, self.send_sems, self.recv_sems = slot, send_sems, recv_sems

    def across(self, step, core):
        return lax.rem(self.x + step, self.n_x) * 2 + core

    def copy(self, source, origin, part, index, target):
        return pltpu.make_async_remote_copy(
            src_ref=source,
            dst_ref=self.slot(origin, part),
            send_sem=self.send_sems.at[part, index],
            recv_sem=self.recv_sems.at[part, origin],
            device_id={"tp": target},
            device_id_type=MESH,
        )

    def own(self, part, source=None):
        source = self.slot(self.me, part) if source is None else source
        targets = [self.across(s, self.core) for s in range(1, self.n_x)] + [self.sibling]
        return [self.copy(source, self.me, part, i, t) for i, t in enumerate(targets)]

    def send(self, part, source=None):
        for copy in self.own(part, source):
            copy.start()

    def relays(self, part):
        out = []
        for s in range(1, self.n_x):
            origin = self.across(s, self.core)
            out.append(
                self.copy(self.slot(origin, part), origin, part, self.n_x - 1 + s, self.sibling)
            )
        return out

    def relay(self, part):
        for copy in self.relays(part):
            copy.wait_recv()
            copy.start()

    def others(self):
        return [self.sibling] + [self.across(s, 1 - self.core) for s in range(1, self.n_x)]

    def wait_slot(self, part, origin):
        self.copy(self.slot(origin, part), origin, part, 0, self.sibling).wait_recv()

    def wait_rest(self, part):
        for origin in self.others():
            self.wait_slot(part, origin)

    def finish(self, part, source=None):
        for copy in self.own(part, source) + self.relays(part):
            copy.wait_send()


def kernel(
    n_tp, n_sp, head_dim,
    stream, gain, query_w, key_w, value_w, out_w, base,
    out,
    xg, gg, wq, wk, wv, wo, normed, bias, qx, kx, vx, att,
    xs, xr, ats, atr, kvs, kvr, gs, gr, wsem, own_sem,
):
    layers, _, rows, width = xg.shape
    groups = kx.shape[1]
    head_cols = groups * LANES
    per_group = LANES // head_dim
    total_width = n_tp * width
    shift = REACH // rows
    sp = lax.axis_index("sp")
    tp = lax.axis_index("tp")
    relayed = shift == 2 and n_sp % 2 == 0

    weights = []
    for l in range(layers):
        pairs = ((key_w, wk), (value_w, wv), (query_w, wq), (out_w, wo))
        weights.append(
            [pltpu.make_async_copy(s.at[l], d.at[l], wsem.at[l, i]) for i, (s, d) in enumerate(pairs)]
        )
    own_stream = pltpu.make_async_copy(stream, xg.at[0, tp], own_sem.at[0])
    own_gain = pltpu.make_async_copy(gain, gg.at[tp], own_sem.at[1])
    own_stream.start()
    own_gain.start()

    barrier = pltpu.get_barrier_semaphore()
    for d in range(1, n_tp):
        pl.semaphore_signal(
            barrier, inc=1, device_id={"tp": lax.rem(tp + d, n_tp)}, device_id_type=MESH
        )
    count = n_tp - 1
    for d in range(1, shift + 1):

        @pl.when(sp + d < n_sp)
        def _():
            pl.semaphore_signal(barrier, inc=1, device_id={"sp": sp + d}, device_id_type=MESH)

        @pl.when(sp >= d)
        def _():
            pl.semaphore_signal(barrier, inc=1, device_id={"sp": sp - d}, device_id_type=MESH)

        count = count + jnp.where(sp + d < n_sp, 1, 0) + jnp.where(sp >= d, 1, 0)
    for copy in weights[0]:
        copy.start()
    pl.semaphore_wait(barrier, count)

    piece = rows // CHUNKS
    xgather = [
        Gather(
            n_tp,
            lambda j, c, l=l: xg.at[l, j, pl.ds(c * piece, piece)],
            xs.at[l],
            xr.at[l],
        )
        for l in range(layers)
    ]
    agather = [
        Gather(n_tp, lambda j, g, l=l: att.at[l, j, g], ats.at[l], atr.at[l])
        for l in range(layers)
    ]

    def stream_piece(c):
        return stream.at[pl.ds(c * piece, piece)]

    for c in range(CHUNKS):
        xgather[0].send(c, stream_piece(c))
    gain_copies = [
        pltpu.make_async_remote_copy(
            src_ref=gain,
            dst_ref=gg.at[tp],
            send_sem=gs.at[d - 1],
            recv_sem=gr.at[d - 1],
            device_id={"tp": lax.rem(tp + d, n_tp)},
            device_id_type=MESH,
        )
        for d in range(1, n_tp)
    ]
    for copy in gain_copies:
        copy.start()
    for l in range(1, layers):
        for copy in weights[l]:
            copy.start()

    for l in range(layers):
        for d in range(1, shift + 1):

            @pl.when(sp < d)
            def _():
                empty = jnp.zeros((rows, LANES), jnp.bfloat16)
                for g in range(groups):
                    kx[l, g, pl.ds((shift - d) * rows, rows), :] = empty
                    vx[l, g, pl.ds((shift - d) * rows, rows), :] = empty

    wide = base.shape[-1]
    seg_q = lax.broadcasted_iota(jnp.int32, (PAIR, BAND), 0) // SEG
    seg_k = lax.broadcasted_iota(jnp.int32, (PAIR, BAND), 1) // SEG
    seen = (seg_k >= seg_q) & (seg_k <= seg_q + PREV)
    for l in range(layers):
        for g in range(groups):
            for h in range(per_group):
                row = base[l, g * per_group + h : g * per_group + h + 1, :]
                table = pltpu.roll(
                    jnp.broadcast_to(row, (PAIR, wide)), 0, 1, stride=1, stride_axis=0
                )[:, :BAND]
                bias[l, g, h * PAIR : (h + 1) * PAIR, :] = jnp.where(seen, table, masked_score)

    tensors = (kx, vx)

    def halo_copy(l, t, g, from_slot, to_slot, index, target):
        buf = tensors[t]
        return pltpu.make_async_remote_copy(
            src_ref=buf.at[l, g, pl.ds(from_slot * rows, rows)],
            dst_ref=buf.at[l, g, pl.ds(to_slot * rows, rows)],
            send_sem=kvs.at[l, t, g, index],
            recv_sem=kvr.at[l, t, g, to_slot],
            device_id={"sp": target},
            device_id_type=MESH,
        )

    even = lax.rem(sp, 2) == 0
    odd_behind = (lax.rem(sp, 2) == 1) & (sp >= 2)

    def direct_copies(l, t, g):
        out_list = []
        for d in range(shift, 0, -1):
            ok = sp + d < n_sp
            if relayed and d == 1:
                ok = even
            out_list.append((ok, halo_copy(l, t, g, shift, shift - d, d - 1, sp + d)))
        return out_list

    def relay_copy(l, t, g):
        return halo_copy(l, t, g, 0, 1, shift, sp - 1)

    def halo_send(l, t, g):
        for ok, copy in direct_copies(l, t, g):
            pl.when(ok)(copy.start)

    def halo_wait(l, t, g):
        for d in range(shift, 0, -1):
            slot = shift - d

            @pl.when(sp >= d)
            def _():
                halo_copy(l, t, g, slot, slot, 0, lax.rem(sp + 1, n_sp)).wait_recv()

            if relayed and d == 2:
                pl.when(odd_behind)(relay_copy(l, t, g).start)

    own_gain.wait()
    for d in range(1, n_tp):
        pltpu.make_async_remote_copy(
            src_ref=gain,
            dst_ref=gg.at[lax.rem(tp - d + n_tp, n_tp)],
            send_sem=gs.at[d - 1],
            recv_sem=gr.at[d - 1],
            device_id={"tp": lax.rem(tp + d, n_tp)},
            device_id_type=MESH,
        ).wait_recv()
    own_stream.wait()

    lane = lax.broadcasted_iota(jnp.int32, (PAIR, LANES), 1) // head_dim
    scale = head_dim ** (-0.5)

    for l in range(layers):
        gather = xgather[l]
        for c in range(CHUNKS):
            gather.relay(c)
        for c in range(CHUNKS):
            gather.wait_rest(c)
            span = slice(c * piece, (c + 1) * piece)
            squares = jnp.zeros((piece, 1), jnp.float32)
            for j in range(n_tp):
                part = xg[l, j, span, :].astype(jnp.float32)
                squares = squares + jnp.sum(part * part, axis=-1, keepdims=True)
            inverse = lax.rsqrt(squares / total_width + epsilon)
            for j in range(n_tp):
                part = xg[l, j, span, :].astype(jnp.float32) * inverse
                normed[span, j * width : (j + 1) * width] = (
                    part * gg[j, l : l + 1, :]
                ).astype(jnp.bfloat16)

        for t, (buf, mat) in enumerate(((kx, wk), (vx, wv))):
            weights[l][t].wait()
            made = jnp.dot(normed[...], mat[l], preferred_element_type=jnp.float32)
            made = made.astype(jnp.bfloat16)
            for g in range(groups):
                buf[l, g, shift * rows :, :] = made[:, g * LANES : (g + 1) * LANES]
            if t == 0:
                halo_send(l, 0, 0)
        halo_send(l, 1, 0)
        for g in range(1, groups):
            halo_send(l, 0, g)
            halo_send(l, 1, g)
        weights[l][2].wait()
        qx[...] = (
            jnp.dot(normed[...], wq[l], preferred_element_type=jnp.float32) * scale
        ).astype(jnp.bfloat16)

        for g in range(groups):
            for t in range(2):
                halo_wait(l, t, g)
            for b in range(rows // PAIR):
                block = qx[b * PAIR : (b + 1) * PAIR, g * LANES : (g + 1) * LANES]
                stacked = jnp.concatenate(
                    [jnp.where(lane == h, block, jnp.zeros_like(block)) for h in range(per_group)],
                    axis=0,
                )
                keys = kx[l, g, b * PAIR : b * PAIR + BAND, :]
                values = vx[l, g, b * PAIR : b * PAIR + BAND, :]
                position = (
                    sp * rows - REACH + b * PAIR
                    + lax.broadcasted_iota(jnp.int32, (1, BAND), 1)
                )
                hidden = jnp.where(position >= 0, 0.0, masked_score)
                scores = lax.dot_general(
                    stacked, keys, (((1,), (1,)), ((), ())), preferred_element_type=jnp.float32
                )
                scores = scores + bias[l, g] + hidden
                top = jnp.max(scores, axis=-1, keepdims=True)
                grown = jnp.exp(scores - top)
                summed = jnp.sum(grown, axis=-1, keepdims=True)
                mix = jnp.dot(
                    grown.astype(jnp.bfloat16), values, preferred_element_type=jnp.float32
                )
                mix = mix / summed
                chosen = mix[:PAIR]
                for h in range(1, per_group):
                    chosen = jnp.where(lane == h, mix[h * PAIR : (h + 1) * PAIR], chosen)
                att[l, tp, g, b * PAIR : (b + 1) * PAIR, :] = chosen.astype(jnp.bfloat16)
            agather[l].send(g)

        gather = agather[l]
        weights[l][3].wait()

        def mixed_part(j):
            wide_rows = jnp.concatenate([att[l, j, g] for g in range(groups)], axis=1)
            mat = wo[l, pl.ds(pl.multiple_of(j * head_cols, LANES), head_cols), :]
            return jnp.dot(wide_rows, mat, preferred_element_type=jnp.float32)

        total = xg[l, tp].astype(jnp.float32) + mixed_part(tp)
        for g in range(groups):
            gather.relay(g)
        for s in range(1, gather.n_x):
            total = total + mixed_part(gather.across(s, gather.core))
        for origin in gather.others():
            for g in range(groups):
                gather.wait_slot(g, origin)
            total = total + mixed_part(origin)
        result = total.astype(jnp.bfloat16)
        if l + 1 < layers:
            xg[l + 1, tp] = result
            for c in range(CHUNKS):
                xgather[l + 1].send(c)
        else:
            out[...] = result

    for copy in gain_copies:
        copy.wait_send()
    for l in range(layers):
        for c in range(CHUNKS):
            xgather[l].finish(c, stream_piece(c) if l == 0 else None)
        for g in range(groups):
            agather[l].finish(g)
            for t in range(2):
                for ok, copy in direct_copies(l, t, g):
                    pl.when(ok)(copy.wait_send)
                if relayed:
                    pl.when(odd_behind)(relay_copy(l, t, g).wait_send)


def per_device(n_tp, n_sp, stream, norm_gain, query_weight, key_weight, value_weight, out_weight, rel_bias):
    rows, width = stream.shape
    layers, full, head_cols = query_weight.shape
    heads_here = rel_bias.shape[1]
    head_dim = head_cols // heads_here
    groups = head_cols // LANES
    n_x = n_tp // 2
    shift = REACH // rows
    far = rel_bias[:, :, 2 * CLIP :]
    base = jnp.concatenate(
        [
            jnp.broadcast_to(far, (layers, heads_here, REACH - CLIP)),
            rel_bias[:, :, :0:-1],
            jnp.broadcast_to(far, (layers, heads_here, PAIR)),
        ],
        axis=2,
    )
    any_space = pl.BlockSpec(memory_space=pl.ANY)
    vmem = pl.BlockSpec(memory_space=pltpu.VMEM)
    bf16, f32 = jnp.bfloat16, jnp.float32
    dma = pltpu.SemaphoreType.DMA
    return pl.pallas_call(
        functools.partial(kernel, n_tp, n_sp, head_dim),
        out_shape=jax.ShapeDtypeStruct((rows, width), bf16),
        in_specs=[any_space] * 6 + [vmem],
        out_specs=vmem,
        scratch_shapes=[
            pltpu.VMEM((layers, n_tp, rows, width), bf16),
            pltpu.VMEM((n_tp, layers, width), f32),
            pltpu.VMEM((layers, full, head_cols), bf16),
            pltpu.VMEM((layers, full, head_cols), bf16),
            pltpu.VMEM((layers, full, head_cols), bf16),
            pltpu.VMEM((layers, n_tp * head_cols, width), bf16),
            pltpu.VMEM((rows, full), bf16),
            pltpu.VMEM((layers, groups, (LANES // head_dim) * PAIR, BAND), f32),
            pltpu.VMEM((rows, head_cols), bf16),
            pltpu.VMEM((layers, groups, REACH + rows, LANES), bf16),
            pltpu.VMEM((layers, groups, REACH + rows, LANES), bf16),
            pltpu.VMEM((layers, n_tp, groups, rows, LANES), bf16),
            dma((layers, CHUNKS, 2 * n_x - 1)),
            dma((layers, CHUNKS, n_tp)),
            dma((layers, groups, 2 * n_x - 1)),
            dma((layers, groups, n_tp)),
            dma((layers, 2, groups, shift + 1)),
            dma((layers, 2, groups, shift)),
            dma((n_tp - 1,)),
            dma((n_tp - 1,)),
            dma((layers, 4)),
            dma((2,)),
        ],
        compiler_params=pltpu.CompilerParams(
            collective_id=0, has_side_effects=True, vmem_limit_bytes=60 * 1024 * 1024
        ),
    )(stream, norm_gain, query_weight, key_weight, value_weight, out_weight, base)


def solution(mesh):
    placed = (
        P("sp", "tp"),
        P(None, "tp"),
        P(None, None, "tp"),
        P(None, None, "tp"),
        P(None, None, "tp"),
        P(None, None, "tp"),
        P(None, "tp", None),
    )
    return jax.shard_map(
        functools.partial(per_device, mesh.shape["tp"], mesh.shape["sp"]),
        mesh=mesh, in_specs=placed, out_specs=P("sp", "tp"), check_vma=False,
    )
```

time: 264 us -> 61.2 us (0.23)
  local copies, waits for them, and re-layouts: 155 us -> 3.55 us
  Pallas kernels: 0 us -> 56.8 us
  matrix products: 31.3 us -> 0 us
  blocking collectives: 27.1 us -> 0 us
  between operations: 15.7 us -> 0.01 us
  waiting for transfers between devices: 14.4 us -> 0 us
  starting transfers between devices: 11.7 us -> 0 us
  other arithmetic: 6.69 us -> 0.62 us
    unnamed x222 -> x1, local copies, waits for them, and re-layouts: 59.2 us -> 1.67 us
    pallas_call x0 -> x1, Pallas kernels: none -> 56.8 us  [per_device(): pl.pallas_call(functools.partial(kernel, n_tp, n_sp, head_dim), out_shape...]
    another operation x256 -> x0, local copies, waits for them, and re-layouts: 52.5 us -> none  [bias_table(): return jnp.stack(slices, axis=1)]
    concatenate x77 -> x0, local copies, waits for them, and re-layouts: 37.9 us -> none  [band_blocks(): jnp.concatenate([blocked[offset_seg:offset_seg + segments] for offset_seg...]
    dot_general x10 -> x0, matrix products: 24 us -> none  [the longest x2 6.3 us: project_rows(): key_sum = jnp.dot(piece, key_mat, preferred_element_type=jnp.float32)]
    all_gather x2 -> x0, blocking collectives: 16.2 us -> none  [per_device(): lax.all_gather(attended, 'tp', axis=1, tiled=True)]
    all_gather x2 -> x0, waiting for transfers between devices: 14.4 us -> none  [project_rows(): piece = lax.all_gather(rows_local, 'tp', axis=1, tiled=True)]
    ppermute x4 -> x0, starting transfers between devices: 11.5 us -> none  [from_behind(): return lax.ppermute(shard, axis, pairs)]
  transfers between devices with their start and end apart: 6 -> 0, of which waited for: 1 -> 0; matrix products, arithmetic and copies ran while one was open for 44% -> 0% of each run, Pallas kernels for 0% -> 0%
where the time goes in v1:
time: 61.2 us; the launch traced here: 60.9 us
  Pallas kernels  56.8 us (93%)
  local copies, waits for them, and re-layouts  3.55 us (6%)
  other arithmetic  0.62 us (1%)
    pallas_call x1, Pallas kernels, per_device(): pl.pallas_call(functools.partial(kernel, n_tp, n_sp, head_dim), out_shape...  56.8 us
    unnamed x1, local copies, waits for them, and re-layouts  1.67 us

profile of v1, /device:TPU:9, one launch (start us, length us, event | category | flops | bytes accessed | tf_op | source)
XLA Modules:
  0.0 60.9 jit_solution(4356066547770222436)
XLA Ops:
  0.0 0.8 %slice_reduce_fusion = f32[2,4]{1,0:T(2,128)S(1)} fusion(f32[2,4,257]{2,1,0:T(4,128)} %param.13), kind=kLoop, calls=%fused_computation.1 | loop fusion | bytes 64 | tf_op jit(solution)/shard_map/slice | solution.py:366
  0.8 0.1 broadcast_in_dim.14
  0.8 0.8 %slice.7 = f32[2,4,256]{2,1,0:T(4,128)S(1)} slice(f32[2,4,257]{2,1,0:T(4,128)} %param.13), slice={[0:2], [0:4], [1:257]} | slice | bytes 16384 | tf_op jit(solution)/shard_map/slice | solution.py:370
  1.6 0.2 rev.3
  1.8 0.1 broadcast_in_dim.13
  1.9 0.6 %pad_maximum_fusion.base = f32[2,4,768]{2,1,0:T(4,128)} fusion(f32[2,4,128]{2,1,0:T(4,128)S(1)} %broadcast_in_dim.14, f32[2,4,256]{2,1,0:T(4,128)S(1)} %rev.3, f32[2,4,384]{2,1,0:T(4,128)S(1)} %broadcast_in_dim.13), kind=kLoop, calls=%fused_computation | loop fusion | flops 12288 | bytes 49152 | tf_op jit(solution)/shard_map/concatenate | solution.py:367
  2.5 56.8 %shard_map.73 = bf16[256,512]{1,0:T(8,128)(2,1)} custom-call(bf16[256,512]{1,0:T(8,128)(2,1)} %stream.1, f32[2,512]{1,0:T(2,128)} %gain.1, bf16[2,2048,256]{2,1,0:T(8,128)(2,1)} %query_w.1, bf16[2,2048,256]{2,1,0:T(8,128)(2,1)} %key_w.1, bf16[2,2048,256]{2,1,0:T(8,128)(2,1)} %value_w.1, bf16[2,1024,512]{2,1,0:T(8,128)(2,1)} %out_w.1, ...), custom_call_target="tpu_custom_call" | custom-call | tf_op jit(solution)/shard_map/pallas_call | solution.py:379
  59.3 1.7 %copy.9 = bf16[256,512]{1,0:T(8,128)(2,1)} copy(bf16[256,512]{1,0:T(8,128)(2,1)} %shard_map.73) | data formatting | bytes 524288

commit v2 on v1

v2 whole, which is shorter than its diff:
```python
import functools

import jax
import jax.numpy as jnp
from jax import lax
from jax.experimental import pallas as pl
from jax.experimental.pallas import tpu as pltpu
from jax.sharding import PartitionSpec as P

SEG = 64
PREV = 8
CLIP = 128
LANES = 128
CHUNKS = 4
PAIR = 2 * SEG
REACH = PREV * SEG
BAND = REACH + PAIR

epsilon = 1e-06
masked_score = -1e30
MESH = pl.DeviceIdType.MESH


class Gather:
    def __init__(self, n_tp, slot, send_sems, recv_sems):
        self.n_x = n_tp // 2
        self.me = lax.axis_index("tp")
        self.core = lax.rem(self.me, 2)
        self.x = self.me // 2
        self.sibling = self.me + 1 - 2 * self.core
        self.slot, self.send_sems, self.recv_sems = slot, send_sems, recv_sems

    def across(self, step, core):
        return lax.rem(self.x + step, self.n_x) * 2 + core

    def copy(self, source, origin, part, index, target):
        return pltpu.make_async_remote_copy(
            src_ref=source,
            dst_ref=self.slot(origin, part),
            send_sem=self.send_sems.at[part, index],
            recv_sem=self.recv_sems.at[part, origin],
            device_id={"tp": target},
            device_id_type=MESH,
        )

    def own(self, part, source=None):
        source = self.slot(self.me, part) if source is None else source
        targets = [self.across(s, self.core) for s in range(1, self.n_x)] + [self.sibling]
        return [self.copy(source, self.me, part, i, t) for i, t in enumerate(targets)]

    def send(self, part, source=None):
        for copy in self.own(part, source):
            copy.start()

    def relays(self, part):
        out = []
        for s in range(1, self.n_x):
            origin = self.across(s, self.core)
            out.append(
                self.copy(self.slot(origin, part), origin, part, self.n_x - 1 + s, self.sibling)
            )
        return out

    def relay(self, part):
        for copy in self.relays(part):
            copy.wait_recv()
            copy.start()

    def others(self):
        return [self.sibling] + [self.across(s, 1 - self.core) for s in range(1, self.n_x)]

    def wait_slot(self, part, origin):
        self.copy(self.slot(origin, part), origin, part, 0, self.sibling).wait_recv()

    def wait_rest(self, part):
        for origin in self.others():
            self.wait_slot(part, origin)

    def finish(self, part, source=None):
        for copy in self.own(part, source) + self.relays(part):
            copy.wait_send()


def kernel(
    n_tp, n_sp, head_dim,
    stream, gain, query_w, key_w, value_w, out_w, rel_bias,
    out,
    xg, gg, table, wq, wk, wv, wo, normed, bias, qx, kx, vx, att,
    xs, xr, ats, atr, kvs, kvr, gs, gr, wsem, own_sem,
):
    layers, _, rows, width = xg.shape
    groups = kx.shape[1]
    head_cols = groups * LANES
    per_group = LANES // head_dim
    total_width = n_tp * width
    shift = REACH // rows
    sp = lax.axis_index("sp")
    tp = lax.axis_index("tp")
    relayed = shift == 2 and n_sp % 2 == 0
    blocks = rows // PAIR
    per_block = CHUNKS // blocks

    weights = []
    for l in range(layers):
        pairs = ((key_w, wk), (value_w, wv), (query_w, wq), (out_w, wo))
        weights.append(
            [pltpu.make_async_copy(s.at[l], d.at[l], wsem.at[l, i]) for i, (s, d) in enumerate(pairs)]
        )
    own_stream = pltpu.make_async_copy(stream, xg.at[0, tp], own_sem.at[0])
    own_gain = pltpu.make_async_copy(gain, gg.at[tp], own_sem.at[1])
    own_stream.start()
    own_gain.start()
    own_table = pltpu.make_async_copy(rel_bias, table, own_sem.at[2])
    own_table.start()

    barrier = pltpu.get_barrier_semaphore()
    for d in range(1, n_tp):
        pl.semaphore_signal(
            barrier, inc=1, device_id={"tp": lax.rem(tp + d, n_tp)}, device_id_type=MESH
        )
    count = n_tp - 1
    for d in range(1, shift + 1):

        @pl.when(sp + d < n_sp)
        def _():
            pl.semaphore_signal(barrier, inc=1, device_id={"sp": sp + d}, device_id_type=MESH)

        @pl.when(sp >= d)
        def _():
            pl.semaphore_signal(barrier, inc=1, device_id={"sp": sp - d}, device_id_type=MESH)

        count = count + jnp.where(sp + d < n_sp, 1, 0) + jnp.where(sp >= d, 1, 0)
    for copy in weights[0]:
        copy.start()
    pl.semaphore_wait(barrier, count)

    piece = rows // CHUNKS
    xgather = [
        Gather(
            n_tp,
            lambda j, c, l=l: xg.at[l, j, pl.ds(c * piece, piece)],
            xs.at[l],
            xr.at[l],
        )
        for l in range(layers)
    ]
    agather = [
        Gather(n_tp, lambda j, b, l=l: att.at[l, j, b], ats.at[l], atr.at[l])
        for l in range(layers)
    ]

    def stream_piece(c):
        return stream.at[pl.ds(c * piece, piece)]

    for c in range(CHUNKS):
        xgather[0].send(c, stream_piece(c))
    gain_copies = [
        pltpu.make_async_remote_copy(
            src_ref=gain,
            dst_ref=gg.at[tp],
            send_sem=gs.at[d - 1],
            recv_sem=gr.at[d - 1],
            device_id={"tp": lax.rem(tp + d, n_tp)},
            device_id_type=MESH,
        )
        for d in range(1, n_tp)
    ]
    for copy in gain_copies:
        copy.start()
    for l in range(1, layers):
        for copy in weights[l]:
            copy.start()

    for l in range(layers):
        for d in range(1, shift + 1):

            @pl.when(sp < d)
            def _():
                empty = jnp.zeros((rows, LANES), jnp.bfloat16)
                for g in range(groups):
                    kx[l, g, pl.ds((shift - d) * rows, rows), :] = empty
                    vx[l, g, pl.ds((shift - d) * rows, rows), :] = empty

    own_table.wait()
    near = 2 * CLIP
    flip = (
        lax.broadcasted_iota(jnp.int32, (near, near), 0)
        + lax.broadcasted_iota(jnp.int32, (near, near), 1)
        == near - 1
    ).astype(jnp.float32)
    seg_q = lax.broadcasted_iota(jnp.int32, (PAIR, BAND), 0) // SEG
    seg_k = lax.broadcasted_iota(jnp.int32, (PAIR, BAND), 1) // SEG
    seen = (seg_k >= seg_q) & (seg_k <= seg_q + PREV)
    for l in range(layers):
        heads = table.shape[1]
        turned = jnp.dot(
            table[l][:, 1:], flip, precision=lax.Precision.HIGHEST,
            preferred_element_type=jnp.float32,
        )
        far = table[l][:, near:]
        base = jnp.concatenate(
            [
                jnp.broadcast_to(far, (heads, REACH - CLIP)),
                turned,
                jnp.broadcast_to(far, (heads, PAIR)),
            ],
            axis=1,
        )
        for h in range(heads):
            spread = jnp.broadcast_to(base[h : h + 1], (PAIR, base.shape[1]))
            shifted = pltpu.roll(spread, 0, 1, stride=1, stride_axis=0)[:, :BAND]
            first = h % per_group * PAIR
            bias[l, h // per_group, first : first + PAIR, :] = jnp.where(
                seen, shifted, masked_score
            )

    tensors = (kx, vx)

    def halo_copy(l, t, g, half, from_slot, to_slot, index, target):
        buf = tensors[t]
        return pltpu.make_async_remote_copy(
            src_ref=buf.at[l, g, pl.ds(from_slot * rows + half * PAIR, PAIR)],
            dst_ref=buf.at[l, g, pl.ds(to_slot * rows + half * PAIR, PAIR)],
            send_sem=kvs.at[l, t, g * blocks + half, index],
            recv_sem=kvr.at[l, t, g * blocks + half, to_slot],
            device_id={"sp": target},
            device_id_type=MESH,
        )

    even = lax.rem(sp, 2) == 0
    odd_behind = (lax.rem(sp, 2) == 1) & (sp >= 2)

    def direct_copies(l, t, g, half):
        out_list = []
        for d in range(shift, 0, -1):
            ok = sp + d < n_sp
            if relayed and d == 1:
                ok = even
            out_list.append((ok, halo_copy(l, t, g, half, shift, shift - d, d - 1, sp + d)))
        return out_list

    def relay_copy(l, t, g, half):
        return halo_copy(l, t, g, half, 0, 1, shift, sp - 1)

    def halo_send(l, half):
        for g in range(groups):
            for t in range(2):
                for ok, copy in direct_copies(l, t, g, half):
                    pl.when(ok)(copy.start)

    def halo_wait_slot(l, t, g, half, d):
        @pl.when(sp >= d)
        def _():
            slot = shift - d
            halo_copy(l, t, g, half, slot, slot, 0, lax.rem(sp + 1, n_sp)).wait_recv()

    def halo_far(l, g, half):
        for t in range(2):
            halo_wait_slot(l, t, g, half, shift)
            if relayed:
                pl.when(odd_behind)(relay_copy(l, t, g, half).start)

    def halo_near(l, g, half):
        for t in range(2):
            for d in range(shift - 1, 0, -1):
                halo_wait_slot(l, t, g, half, d)

    own_gain.wait()
    for d in range(1, n_tp):
        pltpu.make_async_remote_copy(
            src_ref=gain,
            dst_ref=gg.at[lax.rem(tp - d + n_tp, n_tp)],
            send_sem=gs.at[d - 1],
            recv_sem=gr.at[d - 1],
            device_id={"tp": lax.rem(tp + d, n_tp)},
            device_id_type=MESH,
        ).wait_recv()
    own_stream.wait()

    lane = lax.broadcasted_iota(jnp.int32, (PAIR, LANES), 1) // head_dim
    scale = head_dim ** (-0.5)

    def normalize(l, c):
        span = slice(c * piece, (c + 1) * piece)
        squares = jnp.zeros((piece, 1), jnp.float32)
        for j in range(n_tp):
            part = xg[l, j, span, :].astype(jnp.float32)
            squares = squares + jnp.sum(part * part, axis=-1, keepdims=True)
        inverse = lax.rsqrt(squares / total_width + epsilon)
        for j in range(n_tp):
            part = xg[l, j, span, :].astype(jnp.float32) * inverse
            normed[span, j * width : (j + 1) * width] = (
                part * gg[j, l : l + 1, :]
            ).astype(jnp.bfloat16)

    def block_rows(b):
        return slice(b * PAIR, (b + 1) * PAIR)

    def keys_values(l, b):
        for t, (buf, mat) in enumerate(((kx, wk), (vx, wv))):
            if b == 0:
                weights[l][t].wait()
            made = jnp.dot(normed[block_rows(b), :], mat[l], preferred_element_type=jnp.float32)
            made = made.astype(jnp.bfloat16)
            first = shift * rows + b * PAIR
            for g in range(groups):
                buf[l, g, first : first + PAIR, :] = made[:, g * LANES : (g + 1) * LANES]

    def attend(l, b, g):
        lanes = slice(g * LANES, (g + 1) * LANES)
        block = qx[block_rows(b), lanes]
        stacked = jnp.concatenate(
            [jnp.where(lane == h, block, jnp.zeros_like(block)) for h in range(per_group)], axis=0
        )
        keys = kx[l, g, b * PAIR : b * PAIR + BAND, :]
        values = vx[l, g, b * PAIR : b * PAIR + BAND, :]
        position = sp * rows - REACH + b * PAIR + lax.broadcasted_iota(jnp.int32, (1, BAND), 1)
        hidden = jnp.where(position >= 0, 0.0, masked_score)
        scores = lax.dot_general(
            stacked, keys, (((1,), (1,)), ((), ())), preferred_element_type=jnp.float32
        )
        scores = scores + bias[l, g] + hidden
        top = jnp.max(scores, axis=-1, keepdims=True)
        grown = jnp.exp(scores - top)
        summed = jnp.sum(grown, axis=-1, keepdims=True)
        mix = jnp.dot(grown.astype(jnp.bfloat16), values, preferred_element_type=jnp.float32)
        mix = mix / summed
        chosen = mix[:PAIR]
        for h in range(1, per_group):
            chosen = jnp.where(lane == h, mix[h * PAIR : (h + 1) * PAIR], chosen)
        att[l, tp, b, :, lanes] = chosen.astype(jnp.bfloat16)

    def mixed_part(l, b, j):
        mat = wo[l, pl.ds(pl.multiple_of(j * head_cols, LANES), head_cols), :]
        return jnp.dot(att[l, j, b], mat, preferred_element_type=jnp.float32)

    for l in range(layers):
        gather = xgather[l]
        gather.relay(0)
        for b in range(blocks):
            for c in range(b * per_block, (b + 1) * per_block):
                if c + 1 < CHUNKS:
                    gather.relay(c + 1)
                gather.wait_rest(c)
                normalize(l, c)
            keys_values(l, b)
            halo_send(l, b)
        weights[l][2].wait()
        for b in range(blocks):
            if b + 1 < blocks:
                for g in range(groups):
                    halo_far(l, g, b)
            qx[block_rows(b), :] = (
                jnp.dot(normed[block_rows(b), :], wq[l], preferred_element_type=jnp.float32) * scale
            ).astype(jnp.bfloat16)
        for g in range(groups):
            halo_far(l, g, blocks - 1)
        for b in range(blocks):
            for g in range(groups):
                if b == 0:
                    for half in range(blocks):
                        halo_near(l, g, half)
                attend(l, b, g)
            agather[l].send(b)

        gather = agather[l]
        weights[l][3].wait()
        gather.relay(0)
        for b in range(blocks):
            total = xg[l, tp, block_rows(b), :].astype(jnp.float32) + mixed_part(l, b, tp)
            for s in range(1, gather.n_x):
                total = total + mixed_part(l, b, gather.across(s, gather.core))
            if b + 1 < blocks:
                gather.relay(b + 1)
            for origin in gather.others():
                gather.wait_slot(b, origin)
                total = total + mixed_part(l, b, origin)
            result = total.astype(jnp.bfloat16)
            if l + 1 < layers:
                xg[l + 1, tp, block_rows(b), :] = result
                for c in range(b * per_block, (b + 1) * per_block):
                    xgather[l + 1].send(c)
            else:
                out[block_rows(b), :] = result

    for copy in gain_copies:
        copy.wait_send()
    for l in range(layers):
        for c in range(CHUNKS):
            xgather[l].finish(c, stream_piece(c) if l == 0 else None)
        for b in range(blocks):
            agather[l].finish(b)
            for g in range(groups):
                for t in range(2):
                    for ok, copy in direct_copies(l, t, g, b):
                        pl.when(ok)(copy.wait_send)
                    if relayed:
                        pl.when(odd_behind)(relay_copy(l, t, g, b).wait_send)


def per_device(n_tp, n_sp, stream, norm_gain, query_weight, key_weight, value_weight, out_weight, rel_bias):
    rows, width = stream.shape
    layers, full, head_cols = query_weight.shape
    heads_here = rel_bias.shape[1]
    head_dim = head_cols // heads_here
    groups = head_cols // LANES
    n_x = n_tp // 2
    shift = REACH // rows
    blocks = rows // PAIR
    any_space = pl.BlockSpec(memory_space=pl.ANY)
    vmem = pl.BlockSpec(memory_space=pltpu.VMEM)
    bf16, f32 = jnp.bfloat16, jnp.float32
    dma = pltpu.SemaphoreType.DMA
    return pl.pallas_call(
        functools.partial(kernel, n_tp, n_sp, head_dim),
        out_shape=jax.ShapeDtypeStruct((rows, width), bf16),
        in_specs=[any_space] * 7,
        out_specs=vmem,
        scratch_shapes=[
            pltpu.VMEM((layers, n_tp, rows, width), bf16),
            pltpu.VMEM((n_tp, layers, width), f32),
            pltpu.VMEM(rel_bias.shape, f32),
            pltpu.VMEM((layers, full, head_cols), bf16),
            pltpu.VMEM((layers, full, head_cols), bf16),
            pltpu.VMEM((layers, full, head_cols), bf16),
            pltpu.VMEM((layers, n_tp * head_cols, width), bf16),
            pltpu.VMEM((rows, full), bf16),
            pltpu.VMEM((layers, groups, (LANES // head_dim) * PAIR, BAND), f32),
            pltpu.VMEM((rows, head_cols), bf16),
            pltpu.VMEM((layers, groups, REACH + rows, LANES), bf16),
            pltpu.VMEM((layers, groups, REACH + rows, LANES), bf16),
            pltpu.VMEM((layers, n_tp, blocks, PAIR, head_cols), bf16),
            dma((layers, CHUNKS, 2 * n_x - 1)),
            dma((layers, CHUNKS, n_tp)),
            dma((layers, blocks, 2 * n_x - 1)),
            dma((layers, blocks, n_tp)),
            dma((layers, 2, groups * blocks, shift + 1)),
            dma((layers, 2, groups * blocks, shift)),
            dma((n_tp - 1,)),
            dma((n_tp - 1,)),
            dma((layers, 4)),
            dma((3,)),
        ],
        compiler_params=pltpu.CompilerParams(
            collective_id=0, has_side_effects=True, vmem_limit_bytes=60 * 1024 * 1024
        ),
    )(stream, norm_gain, query_weight, key_weight, value_weight, out_weight, rel_bias)


def solution(mesh):
    placed = (
        P("sp", "tp"),
        P(None, "tp"),
        P(None, None, "tp"),
        P(None, None, "tp"),
        P(None, None, "tp"),
        P(None, None, "tp"),
        P(None, "tp", None),
    )
    return jax.shard_map(
        functools.partial(per_device, mesh.shape["tp"], mesh.shape["sp"]),
        mesh=mesh, in_specs=placed, out_specs=P("sp", "tp"), check_vma=False,
    )
```

time: 61.2 us -> 53.6 us (0.88)
  Pallas kernels: 56.8 us -> 51.4 us
  local copies, waits for them, and re-layouts: 3.55 us -> 1.67 us
  other arithmetic: 0.62 us -> 0 us
    pallas_call x1, Pallas kernels: 56.8 us -> 51.4 us  [per_device(): pl.pallas_call(functools.partial(kernel, n_tp, n_sp, head_dim), out_shape...]
    slice x2 -> x0, local copies, waits for them, and re-layouts: 1.55 us -> none  [the longest x1 0.78 us: per_device(): rel_bias[:, :, :0:-1]]
    concatenate x1 -> x0, other arithmetic: 0.62 us -> none  [per_device(): jnp.concatenate([jnp.broadcast_to(far, (layers, heads_here, REACH - CLIP)...]
where the time goes in v2:
time: 53.6 us; the launch traced here: 53.1 us
  Pallas kernels  51.4 us (96%)
  local copies, waits for them, and re-layouts  1.67 us (3%)
    pallas_call x1, Pallas kernels, per_device(): pl.pallas_call(functools.partial(kernel, n_tp, n_sp, head_dim), out_shape...  51.4 us
    unnamed x1, local copies, waits for them, and re-layouts  1.67 us

profile of v2, /device:TPU:9, one launch (start us, length us, event | category | flops | bytes accessed | tf_op | source)
XLA Modules:
  0.0 53.1 jit_solution(7643916021506990468)
XLA Ops:
  0.0 51.4 %shard_map.73 = bf16[256,512]{1,0:T(8,128)(2,1)} custom-call(bf16[256,512]{1,0:T(8,128)(2,1)} %stream.1, f32[2,512]{1,0:T(2,128)} %gain.1, bf16[2,2048,256]{2,1,0:T(8,128)(2,1)} %query_w.1, bf16[2,2048,256]{2,1,0:T(8,128)(2,1)} %key_w.1, bf16[2,2048,256]{2,1,0:T(8,128)(2,1)} %value_w.1, bf16[2,1024,512]{2,1,0:T(8,128)(2,1)} %out_w.1, f32[2,4,257]{2,1,0:T(4,128)} %rel_bias.1), custom_call_target="tpu_custom_call" | custom-call | tf_op jit(solution)/shard_map/pallas_call | solution.py:414
  51.4 1.7 %copy.9 = bf16[256,512]{1,0:T(8,128)(2,1)} copy(bf16[256,512]{1,0:T(8,128)(2,1)} %shard_map.73) | data formatting | bytes 524288
